TPU v7x, 128 devices: a whole 4x4x4 slice. The times are simulated.
128 devices in a mesh: fs: 16 (over z, x), tp: 8 (over y, core).
Axes of the slice: x: 4, y: 4, z: 4, core: 2. Of those that a mesh axis runs over, the one named last changes fastest.
Arguments:
- query_rows: bfloat16 [32768, 2048], P('fs', 'tp'), may hold values from -16 to 16
- key_rows: bfloat16 [32768, 2048], P('fs', 'tp'), may hold values from -8 to 8
- value_rows: bfloat16 [32768, 2048], P('fs', 'tp'), may hold values from -6 to 6
- mix_lambda: float32 [16], P('tp'), may hold values from 0.3 to 0.8
- head_gain: float32 [128], replicated, may hold values from 0.1 to 1.9
- out_cotangent: bfloat16 [32768, 2048], P('fs'), may hold values from -0.049804688 to 0.049804688
- layer_input: bfloat16 [32768, 2048], P('fs'), may hold values from -6 to 6
- value_cotangent: bfloat16 [32768, 2048], P('fs', 'tp'), may hold values from -0.049804688 to 0.049804688
- out_weight: float32 [2048, 2048], P('tp', 'fs'), may hold values from -0.125 to 0.125
- value_weight: float32 [2048, 2048], P('fs', 'tp'), may hold values from -0.125 to 0.125
- out_basis: bfloat16 [2048, 256], replicated, may hold values from -0.125 to 0.125
- value_basis: bfloat16 [2048, 256], replicated, may hold values from -0.125 to 0.125
- out_first: float32 [256, 2048], P('fs', 'tp'), may hold values from -20 to 20
- out_second: float32 [256, 2048], P('fs', 'tp'), may hold values from 0.02 to 0.5
- value_first: float32 [256, 2048], P('fs', 'tp'), may hold values from -20 to 20
- value_second: float32 [256, 2048], P('fs', 'tp'), may hold values from 0.02 to 0.5
Outputs:
- out_step: float32 [2048, 2048], P('tp', 'fs')
- value_step: float32 [2048, 2048], P('fs', 'tp')
- new_out_weight: float32 [2048, 2048], P('tp', 'fs')
- new_value_weight: float32 [2048, 2048], P('fs', 'tp')
- out_copy: bfloat16 [2048, 2048], P('tp')
- value_copy: bfloat16 [2048, 2048], P(None, 'tp')
- new_out_first: float32 [256, 2048], P('fs', 'tp')
- new_out_second: float32 [256, 2048], P('fs', 'tp')
- new_value_first: float32 [256, 2048], P('fs', 'tp')
- new_value_second: float32 [256, 2048], P('fs', 'tp')
All inputs are finite; a program needn't handle non-finite values.
Results may differ from a plain program's by a relative error of at most 0.001.
Values may be sent and summed in bfloat16 or wider, within the bound.
A program may use at most 128 MiB of HBM per device.

v0:
```python
import functools
import math

import jax
import jax.numpy as jnp
from jax import lax
from jax.sharding import Mesh
from jax.sharding import PartitionSpec as P

DH = 64
DV = 128
FS = ("fs_0", "fs_1")
FS_TP = ("fs_0", "fs_1", "tp_0", "tp_1")
TP = ("tp_0", "tp_1")


EPSILON_NORM = 1e-05
EPSILON_ADAM = 1e-08
BETA_ONE = 0.9
BETA_TWO = 0.95
CLIP_RMS = 1.0
LEARN_RATE = 0.01


def in_blocks(value, dim, count):
    lengths = value.shape
    tiles = value.reshape(*lengths[:dim], count, lengths[dim] // count, *lengths[dim + 1 :])
    return jnp.moveaxis(tiles, dim, 0)


def sum_at_owner(value, axis, dim):
    count = lax.axis_size(axis)
    tiles = lax.all_to_all(in_blocks(value, dim, count), axis, 0, 0, tiled=True)
    return jnp.sum(tiles, axis=0)


def by_axis(value, axes):
    return functools.reduce(lax.psum, axes, value)


def sent_together(arrays, axis, dim, along):
    both = jnp.concatenate(arrays, axis=along)
    filled, at, gathered = (lax.all_gather(both, axis, axis=dim, tiled=True), 0, [])
    for a in arrays:
        gathered.append(lax.slice_in_dim(filled, at, at + a.shape[along], axis=along))
        at += a.shape[along]
    return tuple(gathered)


def in_order(tiles, dim):
    tiles = jnp.moveaxis(tiles, 0, dim)
    lengths = tiles.shape
    return tiles.reshape(*lengths[:dim], lengths[dim] * lengths[dim + 1], *lengths[dim + 2 :])


def sent_to_all(value, axis):
    count = lax.axis_size(axis)
    return lax.all_to_all(
        jnp.broadcast_to(value[None], (count, *value.shape)), axis, 0, 0, tiled=True
    )


def gathered_copies(value, axis, dim):
    return in_order(sent_to_all(value, axis), dim)


def attend_blocks(query_rows, key_rows, value_rows, mix_lambda, head_gain):
    seq_len = query_rows.shape[0]
    head_count = mix_lambda.shape[0]
    span_rows = min(512, seq_len)
    query_four = query_rows.reshape(seq_len, head_count, 2, DH)
    key_four = key_rows.reshape(seq_len, head_count, 2, DH)
    value_three = value_rows.reshape(seq_len, head_count, DV)
    key_pos = lax.iota(jnp.int32, seq_len)

    def one_block(block_index):
        row_start = block_index * span_rows
        query_block = lax.dynamic_slice_in_dim(query_four, row_start, span_rows, 0)
        scores = jnp.einsum(
            "qhmd,khmd->hmqk", query_block, key_four, preferred_element_type=jnp.float32
        ) * DH ** (-0.5)
        query_pos = row_start + lax.iota(jnp.int32, span_rows)
        causal = key_pos[None, :] <= query_pos[:, None]
        scores = jnp.where(causal, scores, -jnp.inf)
        row_peak = jnp.max(scores, axis=-1, keepdims=True)
        exp_scores = jnp.exp(scores - row_peak)
        soft_maps = exp_scores / jnp.sum(exp_scores, axis=-1, keepdims=True)
        mix_weights = (soft_maps[:, 0] - mix_lambda[:, None, None] * soft_maps[:, 1]).astype(
            jnp.bfloat16
        )
        raw_out = jnp.einsum(
            "hqk,khv->qhv", mix_weights, value_three, preferred_element_type=jnp.float32
        )
        normed = (
            raw_out
            * lax.rsqrt(jnp.mean(raw_out * raw_out, axis=-1, keepdims=True) + EPSILON_NORM)
            * head_gain
        )
        return normed.astype(jnp.bfloat16).reshape(span_rows, head_count * DV)

    blocks = lax.map(one_block, jnp.arange(seq_len // span_rows))
    return blocks.reshape(seq_len, head_count * DV)


def project_partial(partial_value, basis):
    basis_part = basis.astype(jnp.float32)
    return sum_at_owner(
        jnp.einsum("dr,dv->rv", basis_part, partial_value, precision=lax.Precision.HIGHEST), FS, 0
    )


def moment_step(proj, first, second):
    new_first = BETA_ONE * first + (1.0 - BETA_ONE) * proj
    new_second = BETA_TWO * second + (1.0 - BETA_TWO) * proj * proj
    direction = new_first / (jnp.sqrt(new_second) + EPSILON_ADAM)
    return (new_first, new_second, direction)


def body(
    query_rows,
    key_rows,
    value_rows,
    mix_lambda,
    head_gain,
    out_cotangent,
    layer_input,
    value_cotangent,
    out_weight,
    value_weight,
    out_basis,
    value_basis,
    out_first,
    out_second,
    value_first,
    value_second,
):
    head_out = attend_blocks(query_rows, key_rows, value_rows, mix_lambda, head_gain)
    fs_count = lax.axis_size(FS)
    row_share = out_cotangent.shape[1] // fs_count
    row_base = lax.axis_index(FS) * row_share
    out_rows_b = lax.dynamic_slice_in_dim(out_basis, row_base, row_share, 0).astype(jnp.float32)
    value_rows_b = lax.dynamic_slice_in_dim(value_basis, row_base, row_share, 0).astype(jnp.float32)
    out_partial = jnp.einsum(
        "td,tv->dv", out_cotangent, head_out, preferred_element_type=jnp.float32
    )
    value_partial = jnp.einsum(
        "td,tv->dv", layer_input, value_cotangent, preferred_element_type=jnp.float32
    )
    out_proj = project_partial(out_partial, out_basis)
    value_proj = project_partial(value_partial, value_basis)
    new_out_first, new_out_second, out_dir = moment_step(out_proj, out_first, out_second)
    new_value_first, new_value_second, value_dir = moment_step(
        value_proj, value_first, value_second
    )
    out_sumsq, value_sumsq = (
        by_axis(jnp.sum(out_dir * out_dir), FS_TP),
        by_axis(jnp.sum(value_dir * value_dir), FS_TP),
    )
    entry_count = out_first.shape[0] * fs_count * out_first.shape[1] * lax.axis_size(TP)
    out_clip = jnp.minimum(1.0, CLIP_RMS * math.sqrt(entry_count) / jnp.sqrt(out_sumsq))
    value_clip = jnp.minimum(1.0, CLIP_RMS * math.sqrt(entry_count) / jnp.sqrt(value_sumsq))
    parts = sent_together((out_dir, value_dir), FS, 0, 1)
    out_total = jnp.dot(out_rows_b, parts[0], precision=lax.Precision.HIGHEST)
    value_total = jnp.dot(value_rows_b, parts[1], precision=lax.Precision.HIGHEST)
    value_step = value_clip * value_total
    out_step = (out_clip * out_total).T
    new_value_weight = value_weight - LEARN_RATE * value_step
    new_out_weight = out_weight - LEARN_RATE * out_step
    out_copy, value_copy = (
        gathered_copies(new_out_weight.astype(jnp.bfloat16), FS, 1),
        gathered_copies(new_value_weight.astype(jnp.bfloat16), FS, 0),
    )
    return (
        out_step,
        value_step,
        new_out_weight,
        new_value_weight,
        out_copy,
        value_copy,
        new_out_first,
        new_out_second,
        new_value_first,
        new_value_second,
    )


def solution(mesh):
    torus = Mesh(mesh.devices.reshape(4, 4, 4, 2), ("fs_0", "fs_1", "tp_0", "tp_1"))
    placed = (
        P(FS, TP),
        P(FS, TP),
        P(FS, TP),
        P(TP),
        P(),
        P(FS, None),
        P(FS, None),
        P(FS, TP),
        P(TP, FS),
        P(FS, TP),
        P(),
        P(),
        P(FS, TP),
        P(FS, TP),
        P(FS, TP),
        P(FS, TP),
    )
    return jax.shard_map(
        body,
        mesh=torus,
        in_specs=placed,
        out_specs=(
            P(TP, FS),
            P(FS, TP),
            P(TP, FS),
            P(FS, TP),
            P(TP, None),
            P(None, TP),
            P(FS, TP),
            P(FS, TP),
            P(FS, TP),
            P(FS, TP),
        ),
        check_vma=False,
    )
```

profile of v0, /device:TPU:0, one launch (start us, length us, event | category | flops | bytes accessed | tf_op | source)
XLA Modules:
  0.0 269.9 jit_solution(9044050612719366407)
XLA Ops:
  7.6 125.3 %while.11 = (s32[]{:T(128)}, bf16[4,512,256]{2,1,0:T(8,128)(2,1)S(1)}, s32[4]{0:T(128)S(1)}, bf16[2048,2,2,64]{0,3,2,1:T(8,128)(2,1)}, bf16[2048,2,2,64]{0,3,2,1...) while((s32[]{:T(128)}, ...), condition=%wide.region_4.5_spmd.clone, body=%wide.region_0.4_spmd.clone.sunk | while | flops 1102712320 | bytes 78158648 | solution.py:101
  9.5 10.3 %fusion.69 = (f32[2,2,512]{2,1,0:T(2,128)S(1)}, f32[2,2,512,2048]{3,2,1,0:T(8,128)}) fusion(pred[512,2048]{1,0:T(8,128)(4,1)S(1)} %iota_compare_fusion.2, bf16[2048,2,2,64]{0,3,2,1:T(8,128)(2,1)} %get-tuple-element.213, bf16[2048,2,2,64]{0,3,2,1:T(8,128)(2,1)} %get-tuple-element.212, s32[]{:T(128)S(6)} %select_n.27), kind=kOutput, calls=%fused_computation.53.clone.1 | convolution fusion | flops 553650176 | bytes 19144708 | tf_op jit(solution)/shard_map/while/body/eval_jaxpr/sub | solution.py:86
  19.8 12.0 %broadcast_divide_fusion.2 = f32[2,2,512,2048]{3,2,1,0:T(8,128)} fusion(f32[2,2,512,2048]{3,2,1,0:T(8,128)} %get-tuple-element.181, f32[2,2,512]{2,1,0:T(2,128)S(1)} %get-tuple-element.182), kind=kLoop, calls=%fused_computation.10.clone.1 | loop fusion | flops 4194304 | bytes 33562624 | tf_op jit(solution)/shard_map/while/body/eval_jaxpr/div | solution.py:87
  31.8 6.8 %multiply_reduce_fusion.4 = (f32[512,2]{0,1:T(2,128)S(1)}, f32[512,2,128]{0,2,1:T(8,128)S(1)}) fusion(bf16[2048,2,128]{0,2,1:T(8,128)(2,1)S(1)} %copy-done.3, f32[2,2,512,2048]{3,2,1,0:T(8,128)} %broadcast_divide_fusion.2, f32[2]{0:T(128)S(1)} %copy-done.11), kind=kOutput, calls=%fused_computation.19.clone.1 | convolution fusion | flops 543423488 | bytes 18354184 | tf_op jit(solution)/shard_map/while/body/eval_jaxpr/hqk,khv->qhv/dot_general | solution.py:91
  40.8 10.3 %fusion.69 = (f32[2,2,512]{2,1,0:T(2,128)S(1)}, f32[2,2,512,2048]{3,2,1,0:T(8,128)}) fusion(pred[512,2048]{1,0:T(8,128)(4,1)S(1)} %iota_compare_fusion.2, bf16[2048,2,2,64]{0,3,2,1:T(8,128)(2,1)} %get-tuple-element.213, bf16[2048,2,2,64]{0,3,2,1:T(8,128)(2,1)} %get-tuple-element.212, s32[]{:T(128)S(6)} %select_n.27), kind=kOutput, calls=%fused_computation.53.clone.1 | convolution fusion | flops 553650176 | bytes 19144708 | tf_op jit(solution)/shard_map/while/body/eval_jaxpr/sub | solution.py:86
  51.1 12.0 %broadcast_divide_fusion.2 = f32[2,2,512,2048]{3,2,1,0:T(8,128)} fusion(f32[2,2,512,2048]{3,2,1,0:T(8,128)} %get-tuple-element.181, f32[2,2,512]{2,1,0:T(2,128)S(1)} %get-tuple-element.182), kind=kLoop, calls=%fused_computation.10.clone.1 | loop fusion | flops 4194304 | bytes 33562624 | tf_op jit(solution)/shard_map/while/body/eval_jaxpr/div | solution.py:87
  63.1 6.8 %multiply_reduce_fusion.4 = (f32[512,2]{0,1:T(2,128)S(1)}, f32[512,2,128]{0,2,1:T(8,128)S(1)}) fusion(bf16[2048,2,128]{0,2,1:T(8,128)(2,1)S(1)} %copy-done.3, f32[2,2,512,2048]{3,2,1,0:T(8,128)} %broadcast_divide_fusion.2, f32[2]{0:T(128)S(1)} %copy-done.11), kind=kOutput, calls=%fused_computation.19.clone.1 | convolution fusion | flops 543423488 | bytes 18354184 | tf_op jit(solution)/shard_map/while/body/eval_jaxpr/hqk,khv->qhv/dot_general | solution.py:91
  72.1 10.3 %fusion.69 = (f32[2,2,512]{2,1,0:T(2,128)S(1)}, f32[2,2,512,2048]{3,2,1,0:T(8,128)}) fusion(pred[512,2048]{1,0:T(8,128)(4,1)S(1)} %iota_compare_fusion.2, bf16[2048,2,2,64]{0,3,2,1:T(8,128)(2,1)} %get-tuple-element.213, bf16[2048,2,2,64]{0,3,2,1:T(8,128)(2,1)} %get-tuple-element.212, s32[]{:T(128)S(6)} %select_n.27), kind=kOutput, calls=%fused_computation.53.clone.1 | convolution fusion | flops 553650176 | bytes 19144708 | tf_op jit(solution)/shard_map/while/body/eval_jaxpr/sub | solution.py:86
  82.5 12.0 %broadcast_divide_fusion.2 = f32[2,2,512,2048]{3,2,1,0:T(8,128)} fusion(f32[2,2,512,2048]{3,2,1,0:T(8,128)} %get-tuple-element.181, f32[2,2,512]{2,1,0:T(2,128)S(1)} %get-tuple-element.182), kind=kLoop, calls=%fused_computation.10.clone.1 | loop fusion | flops 4194304 | bytes 33562624 | tf_op jit(solution)/shard_map/while/body/eval_jaxpr/div | solution.py:87
  94.4 6.8 %multiply_reduce_fusion.4 = (f32[512,2]{0,1:T(2,128)S(1)}, f32[512,2,128]{0,2,1:T(8,128)S(1)}) fusion(bf16[2048,2,128]{0,2,1:T(8,128)(2,1)S(1)} %copy-done.3, f32[2,2,512,2048]{3,2,1,0:T(8,128)} %broadcast_divide_fusion.2, f32[2]{0:T(128)S(1)} %copy-done.11), kind=kOutput, calls=%fused_computation.19.clone.1 | convolution fusion | flops 543423488 | bytes 18354184 | tf_op jit(solution)/shard_map/while/body/eval_jaxpr/hqk,khv->qhv/dot_general | solution.py:91
  103.5 10.3 %fusion.69 = (f32[2,2,512]{2,1,0:T(2,128)S(1)}, f32[2,2,512,2048]{3,2,1,0:T(8,128)}) fusion(pred[512,2048]{1,0:T(8,128)(4,1)S(1)} %iota_compare_fusion.2, bf16[2048,2,2,64]{0,3,2,1:T(8,128)(2,1)} %get-tuple-element.213, bf16[2048,2,2,64]{0,3,2,1:T(8,128)(2,1)} %get-tuple-element.212, s32[]{:T(128)S(6)} %select_n.27), kind=kOutput, calls=%fused_computation.53.clone.1 | convolution fusion | flops 553650176 | bytes 19144708 | tf_op jit(solution)/shard_map/while/body/eval_jaxpr/sub | solution.py:86
  113.8 12.0 %broadcast_divide_fusion.2 = f32[2,2,512,2048]{3,2,1,0:T(8,128)} fusion(f32[2,2,512,2048]{3,2,1,0:T(8,128)} %get-tuple-element.181, f32[2,2,512]{2,1,0:T(2,128)S(1)} %get-tuple-element.182), kind=kLoop, calls=%fused_computation.10.clone.1 | loop fusion | flops 4194304 | bytes 33562624 | tf_op jit(solution)/shard_map/while/body/eval_jaxpr/div | solution.py:87
  125.8 6.8 %multiply_reduce_fusion.4 = (f32[512,2]{0,1:T(2,128)S(1)}, f32[512,2,128]{0,2,1:T(8,128)S(1)}) fusion(bf16[2048,2,128]{0,2,1:T(8,128)(2,1)S(1)} %copy-done.3, f32[2,2,512,2048]{3,2,1,0:T(8,128)} %broadcast_divide_fusion.2, f32[2]{0:T(128)S(1)} %copy-done.11), kind=kOutput, calls=%fused_computation.19.clone.1 | convolution fusion | flops 543423488 | bytes 18354184 | tf_op jit(solution)/shard_map/while/body/eval_jaxpr/hqk,khv->qhv/dot_general | solution.py:91
  132.9 5.8 %fusion.47 = f32[256,2048]{1,0:T(8,128)S(1)} fusion(bf16[2048,256]{1,0:T(8,128)(2,1)S(1)} %bitcast.68, bf16[2048,2048]{1,0:T(8,128)(2,1)} %param.23), kind=kOutput, calls=%fused_computation.54 | convolution fusion | flops 2147483648 | bytes 11534336 | tf_op jit(solution)/shard_map/td,tv->dv/dot_general | solution.py:143
  140.9 8.0 %all-to-all-start = ((f32[16,16,256]{2,1,0:T(8,128)}), f32[16,16,256]{2,1,0:T(8,128)S(1)}, u32[]{:S(2)}, u32[]{:S(2)}) async-start(f32[16,16,256]{2,1,0:T(8,128)} %bitcast.5), calls=%async_computation | async-start | bytes 524288 | tf_op jit(solution)/shard_map/all_to_all | solution.py:33
  149.0 6.1 %fusion.49 = f32[2048,256]{1,0:T(8,128)S(1)} fusion(bf16[2048,2048]{1,0:T(8,128)(2,1)} %param.24, bf16[2048,256]{1,0:T(8,128)(2,1)S(1)} %copy-done), kind=kOutput, calls=%fused_computation.56 | convolution fusion | flops 2147483648 | bytes 11534336 | tf_op jit(solution)/shard_map/td,tv->dv/dot_general | solution.py:146
  157.6 6.9 %all-to-all-start.1 = ((f32[16,16,256]{2,1,0:T(8,128)}), f32[16,16,256]{2,1,0:T(8,128)S(1)}, u32[]{:S(2)}, u32[]{:S(2)}) async-start(f32[16,16,256]{2,1,0:T(8,128)} %bitcast.7), calls=%async_computation.1 | async-start | bytes 524288 | tf_op jit(solution)/shard_map/all_to_all | solution.py:33
  165.8 7.4 %all-to-all-done.1 = f32[16,16,256]{2,1,0:T(8,128)S(1)} async-done(((f32[16,16,256]{2,1,0:T(8,128)}), f32[16,16,256]{2,1,0:T(8,128)S(1)}, u32[]{:S(2)}, u32[]{:S(2)}) %all-to-all-start.1) | async-done | bytes 262176 | tf_op jit(solution)/shard_map/all_to_all | solution.py:33
  174.5 9.2 %all-reduce.2 = (f32[]{:T(128)}, f32[]{:T(128)}) all-reduce(f32[]{:T(128)} %get-tuple-element.118, f32[]{:T(128)} %get-tuple-element.114), channel_id=1, replica_groups=mesh['fs_0'=4,'fs_1'=4,'tp_0'=4,'tp_1'=2] {'fs_0'}, use_global_device_ids=true, to_apply=%region_7.8 | all-reduce | flops 2 | bytes 16 | tf_op jit(solution)/shard_map/psum | solution.py:38
  183.7 9.3 %all-reduce.1 = (f32[]{:T(128)}, f32[]{:T(128)}) all-reduce(f32[]{:T(128)} %get-tuple-element.106, f32[]{:T(128)} %get-tuple-element.107), channel_id=1, replica_groups=mesh['fs_0'=4,'fs_1'=4,'tp_0'=4,'tp_1'=2] {'fs_1'}, use_global_device_ids=true, to_apply=%region_8.9 | all-reduce | flops 2 | bytes 16 | tf_op jit(solution)/shard_map/psum | solution.py:38
  193.0 11.3 %all-reduce = (f32[]{:T(128)}, f32[]{:T(128)}) all-reduce(f32[]{:T(128)} %get-tuple-element.104, f32[]{:T(128)} %get-tuple-element.105), channel_id=1, replica_groups=mesh['fs_0'=4,'fs_1'=4,'tp_0'=4,'tp_1'=2] {'tp_0'}, use_global_device_ids=true, to_apply=%region_9.10 | all-reduce | flops 2 | bytes 16 | tf_op jit(solution)/shard_map/psum | solution.py:38
  208.1 21.9 %all_gather.3 = f32[256,512]{1,0:T(8,128)S(1)} all-gather(f32[16,512]{1,0:T(8,128)S(1)} %pad_maximum_fusion), channel_id=1, replica_groups=mesh['fs_0'=4,'fs_1'=4,'tp_0'=4,'tp_1'=2] {'fs_0','fs_1'}, dimensions={0}, use_global_device_ids=true | all-gather | bytes 557056 | tf_op jit(solution)/shard_map/all_gather | solution.py:43
  240.2 10.6 %all-to-all-done.2 = bf16[16,256,128]{2,1,0:T(8,128)(2,1)S(1)} async-done(((bf16[16,256,128]{2,1,0:T(8,128)(2,1)}), bf16[16,256,128]{2,1,0:T(8,128)(2,1)S(1)}, u32[]{:S(2)}, u32[]{:S(2)}) %all-to-all-start.2) | async-done | bytes 1048608 | tf_op jit(solution)/shard_map/all_to_all | solution.py:58
  259.2 9.7 %all-to-all-done.3 = bf16[16,128,256]{2,1,0:T(8,128)(2,1)S(1)} async-done(((bf16[16,128,256]{2,1,0:T(8,128)(2,1)}), bf16[16,128,256]{2,1,0:T(8,128)(2,1)S(1)}, u32[]{:S(2)}, u32[]{:S(2)}) %all-to-all-start.3) | async-done | bytes 1048608 | tf_op jit(solution)/shard_map/all_to_all | solution.py:58
  (93 shorter events, 42.0 us)
Async XLA Ops:
  0.6 148.3 %copy-start = (bf16[2048,256]{1,0:T(8,128)(2,1)S(1)}, bf16[2048,256]{1,0:T(8,128)(2,1)}, u32[]{:S(2)}) copy-start(bf16[2048,256]{1,0:T(8,128)(2,1)} %param.25) | copy-start | bytes 3145732
  19.8 12.0 %copy-start.3 = (bf16[2048,2,128]{0,2,1:T(8,128)(2,1)S(1)}, bf16[2048,2,128]{0,2,1:T(8,128)(2,1)}, u32[]{:S(2)}) copy-start(bf16[2048,2,128]{0,2,1:T(8,128)(2,1)} %get-tuple-element.215) | copy-start | bytes 3145732 | tf_op jit(solution)/shard_map/while
  19.8 12.0 %copy-start.11 = (f32[2]{0:T(128)S(1)}, f32[2]{0:T(128)}, u32[]{:S(2)}) copy-start(f32[2]{0:T(128)} %get-tuple-element.214) | copy-start | bytes 28 | tf_op jit(solution)/shard_map/while
  31.8 6.8 %copy-start.10 = (f32[128]{0:T(128)S(1)}, f32[128]{0:T(128)}, u32[]{:S(2)}) copy-start(f32[128]{0:T(128)} %get-tuple-element.216) | copy-start | bytes 1540 | tf_op jit(solution)/shard_map/while
  51.1 12.0 %copy-start.3 = (bf16[2048,2,128]{0,2,1:T(8,128)(2,1)S(1)}, bf16[2048,2,128]{0,2,1:T(8,128)(2,1)}, u32[]{:S(2)}) copy-start(bf16[2048,2,128]{0,2,1:T(8,128)(2,1)} %get-tuple-element.215) | copy-start | bytes 3145732 | tf_op jit(solution)/shard_map/while
  51.1 12.0 %copy-start.11 = (f32[2]{0:T(128)S(1)}, f32[2]{0:T(128)}, u32[]{:S(2)}) copy-start(f32[2]{0:T(128)} %get-tuple-element.214) | copy-start | bytes 28 | tf_op jit(solution)/shard_map/while
  63.1 6.8 %copy-start.10 = (f32[128]{0:T(128)S(1)}, f32[128]{0:T(128)}, u32[]{:S(2)}) copy-start(f32[128]{0:T(128)} %get-tuple-element.216) | copy-start | bytes 1540 | tf_op jit(solution)/shard_map/while
  82.5 12.0 %copy-start.3 = (bf16[2048,2,128]{0,2,1:T(8,128)(2,1)S(1)}, bf16[2048,2,128]{0,2,1:T(8,128)(2,1)}, u32[]{:S(2)}) copy-start(bf16[2048,2,128]{0,2,1:T(8,128)(2,1)} %get-tuple-element.215) | copy-start | bytes 3145732 | tf_op jit(solution)/shard_map/while
  82.5 12.0 %copy-start.11 = (f32[2]{0:T(128)S(1)}, f32[2]{0:T(128)}, u32[]{:S(2)}) copy-start(f32[2]{0:T(128)} %get-tuple-element.214) | copy-start | bytes 28 | tf_op jit(solution)/shard_map/while
  94.4 6.8 %copy-start.10 = (f32[128]{0:T(128)S(1)}, f32[128]{0:T(128)}, u32[]{:S(2)}) copy-start(f32[128]{0:T(128)} %get-tuple-element.216) | copy-start | bytes 1540 | tf_op jit(solution)/shard_map/while
  113.8 12.0 %copy-start.3 = (bf16[2048,2,128]{0,2,1:T(8,128)(2,1)S(1)}, bf16[2048,2,128]{0,2,1:T(8,128)(2,1)}, u32[]{:S(2)}) copy-start(bf16[2048,2,128]{0,2,1:T(8,128)(2,1)} %get-tuple-element.215) | copy-start | bytes 3145732 | tf_op jit(solution)/shard_map/while
  113.8 12.0 %copy-start.11 = (f32[2]{0:T(128)S(1)}, f32[2]{0:T(128)}, u32[]{:S(2)}) copy-start(f32[2]{0:T(128)} %get-tuple-element.214) | copy-start | bytes 28 | tf_op jit(solution)/shard_map/while
  125.8 6.8 %copy-start.10 = (f32[128]{0:T(128)S(1)}, f32[128]{0:T(128)}, u32[]{:S(2)}) copy-start(f32[128]{0:T(128)} %get-tuple-element.216) | copy-start | bytes 1540 | tf_op jit(solution)/shard_map/while
  140.9 16.7 %all-to-all-start = ((f32[16,16,256]{2,1,0:T(8,128)}), f32[16,16,256]{2,1,0:T(8,128)S(1)}, u32[]{:S(2)}, u32[]{:S(2)}) async-start(f32[16,16,256]{2,1,0:T(8,128)} %bitcast.5), calls=%async_computation | async-start | bytes 524288 | tf_op jit(solution)/shard_map/all_to_all | solution.py:33
  148.9 6.2 %copy-start.2 = (bf16[2048,256]{1,0:T(8,128)(2,1)S(1)}, bf16[2048,256]{1,0:T(8,128)(2,1)}, u32[]{:S(2)}) copy-start(bf16[2048,256]{1,0:T(8,128)(2,1)} %param.29) | copy-start | bytes 3145732
  148.9 15.6 %copy-start.6 = (f32[16,256]{1,0:T(8,128)S(1)}, f32[16,256]{1,0:T(8,128)}, u32[]{:S(2)}) copy-start(f32[16,256]{1,0:T(8,128)} %param.31) | copy-start | bytes 49156
  148.9 15.6 %copy-start.7 = (f32[16,256]{1,0:T(8,128)S(1)}, f32[16,256]{1,0:T(8,128)}, u32[]{:S(2)}) copy-start(f32[16,256]{1,0:T(8,128)} %param.30) | copy-start | bytes 49156
  148.9 24.3 %copy-start.8 = (f32[16,256]{1,0:T(8,128)S(1)}, f32[16,256]{1,0:T(8,128)}, u32[]{:S(2)}) copy-start(f32[16,256]{1,0:T(8,128)} %param.33) | copy-start | bytes 49156
  149.0 24.3 %copy-start.9 = (f32[16,256]{1,0:T(8,128)S(1)}, f32[16,256]{1,0:T(8,128)}, u32[]{:S(2)}) copy-start(f32[16,256]{1,0:T(8,128)} %param.32) | copy-start | bytes 49156
  149.0 81.1 %copy-start.4 = (f32[256,128]{1,0:T(8,128)S(1)}, f32[256,128]{1,0:T(8,128)}, u32[]{:S(2)}) copy-start(f32[256,128]{1,0:T(8,128)} %param.26) | copy-start | bytes 393220
  155.1 83.4 %copy-start.5 = (f32[128,256]{1,0:T(8,128)S(1)}, f32[128,256]{1,0:T(8,128)}, u32[]{:S(2)}) copy-start(f32[128,256]{1,0:T(8,128)} %param.27) | copy-start | bytes 393220
  157.6 15.6 %all-to-all-start.1 = ((f32[16,16,256]{2,1,0:T(8,128)}), f32[16,16,256]{2,1,0:T(8,128)S(1)}, u32[]{:S(2)}, u32[]{:S(2)}) async-start(f32[16,16,256]{2,1,0:T(8,128)} %bitcast.7), calls=%async_computation.1 | async-start | bytes 524288 | tf_op jit(solution)/shard_map/all_to_all | solution.py:33
  233.2 17.7 %all-to-all-start.2 = ((bf16[16,256,128]{2,1,0:T(8,128)(2,1)}), bf16[16,256,128]{2,1,0:T(8,128)(2,1)S(1)}, u32[]{:S(2)}, u32[]{:S(2)}) async-start(bf16[16,256,128]{2,1,0:T(8,128)(2,1)} %broadcast_in_dim.26), calls=%async_computation.2 | async-start | bytes 2097152 | tf_op jit(solution)/shard_map/all_to_all | solution.py:58
  252.0 17.0 %all-to-all-start.3 = ((bf16[16,128,256]{2,1,0:T(8,128)(2,1)}), bf16[16,128,256]{2,1,0:T(8,128)(2,1)S(1)}, u32[]{:S(2)}, u32[]{:S(2)}) async-start(bf16[16,128,256]{2,1,0:T(8,128)(2,1)} %broadcast_in_dim.27), calls=%async_computation.3 | async-start | bytes 2097152 | tf_op jit(solution)/shard_map/all_to_all | solution.py:58
  (1 other events, 5.8 us)
where the time goes:
time: 271 us; the launch traced here: 270 us
  matrix products  88.5 us (33%)
  blocking collectives  54.9 us (20%)
  other arithmetic  53.4 us (20%)
  waiting for transfers between devices  28.1 us (10%)
  starting transfers between devices  23.1 us (9%)
  local copies, waits for them, and re-layouts  16.8 us (6%)
  loops' own time  2.95 us (1%)
    div x4, other arithmetic, one_block(): soft_maps = exp_scores / jnp.sum(exp_scores, axis=-1, keepdims=True)  47.8 us
    sub x4, matrix products, one_block(): exp_scores = jnp.exp(scores - row_peak)  41.3 us
    psum x4, blocking collectives, by_axis(): return functools.reduce(lax.psum, axes, value)  32.9 us
    dot_general x4, matrix products, one_block(): jnp.einsum('hqk,khv->qhv', mix_weights, value_three, preferred_element_ty...  27.2 us
    all_gather x1, blocking collectives, sent_together(): lax.all_gather(both, axis, axis=dim, tiled=True)  21.9 us
    all_to_all x2, waiting for transfers between devices, sent_to_all(): lax.all_to_all(jnp.broadcast_to(value[None], (count, *value.shape)), axis...  20.4 us
    all_to_all x2, starting transfers between devices, sum_at_owner(): tiles = lax.all_to_all(in_blocks(value, dim, count), axis, 0, 0, tiled=True)  14.9 us
    unnamed x23, local copies, waits for them, and re-layouts  10.2 us
  transfers between devices with their start and end apart: 4, of which 4 were waited for; matrix products, arithmetic and copies ran while one was open for 6% of the time, Pallas kernels for 0%

commit v1 on v0

v1 whole, which is shorter than its diff:
```python
import math

import jax
import jax.numpy as jnp
from jax import lax
from jax.experimental import pallas as pl
from jax.experimental.pallas import tpu as pltpu
from jax.sharding import Mesh
from jax.sharding import PartitionSpec as P

FS = ("fs_0", "fs_1")
TP = ("tp_0", "tp_1")

SEQ = 2048
WIDE = 2048
COLS = 256
RANK = 256
BLOCK = 256
FS_SIDE = 4
FS_COUNT = 16
SHARE = RANK // FS_COUNT
OWN = WIDE // FS_COUNT
DH = 64
DV = 128

EPSILON_NORM = 1e-05
EPSILON_ADAM = 1e-08
BETA_ONE = 0.9
BETA_TWO = 0.95
CLIP_RMS = 1.0
LEARN_RATE = 0.01
ENTRY_COUNT = RANK * WIDE
SCORE_SCALE = math.log2(math.e) * DH**-0.5

F32 = jnp.float32
BF16 = jnp.bfloat16
MESH = pl.DeviceIdType.MESH
NT = (((1,), (1,)), ((), ()))
NN = (((1,), (0,)), ((), ()))


def mul(a, b, dims=NN):
    return lax.dot_general(a, b, dims, preferred_element_type=F32)


def two_parts(value):
    high = value.astype(BF16)
    return high, (value - high.astype(F32)).astype(BF16)


def moment_step(proj, first, second):
    new_first = BETA_ONE * first + (1.0 - BETA_ONE) * proj
    new_second = BETA_TWO * second + (1.0 - BETA_TWO) * proj * proj
    direction = new_first / (jnp.sqrt(new_second) + EPSILON_ADAM)
    return (new_first, new_second, direction)


def column(row):
    return jnp.transpose(jnp.broadcast_to(row, (row.shape[1], row.shape[1])))


class Gather:
    def __init__(self, buf, send, recv, z, x):
        self.buf, self.send, self.recv = buf, send, recv
        self.pos = {"fs_0": z, "fs_1": x}
        self.rows = buf.shape[3]

    def at(self, half, where, part):
        rows = slice(None) if part is None else pl.ds(part * (self.rows // 2), self.rows // 2)
        first = where.get("fs_0", slice(None))
        second = where.get("fs_1", slice(None))
        return self.buf.at[first, second, half, rows]

    def copies(self, stage):
        phase, forward = divmod(stage, 2)
        out = []
        for half in range(2):
            order = FS if half == 0 else FS[::-1]
            axis = order[phase]
            other = order[1 - phase]
            for way in range(2):
                step = 1 if way == 0 else FS_SIDE - 1
                here = self.pos[axis]
                target = lax.rem(here + step, FS_SIDE)
                held = here if not forward else lax.rem(here + FS_SIDE - step, FS_SIDE)
                where = {axis: held}
                if phase == 0:
                    where[other] = self.pos[other]
                view = self.at(half, where, way if forward else None)
                index = stage * 4 + half * 2 + way
                out.append(
                    pltpu.make_async_remote_copy(
                        src_ref=view,
                        dst_ref=view,
                        send_sem=self.send.at[index],
                        recv_sem=self.recv.at[index],
                        device_id={axis: target},
                        device_id_type=MESH,
                    )
                )
        return out

    def start(self, stage):
        for copy in self.copies(stage):
            copy.start()

    def arrive(self, stage):
        for copy in self.copies(stage):
            copy.wait_recv()

    def finish(self):
        for stage in range(4):
            for copy in self.copies(stage):
                copy.wait_send()


def spread(z, x):
    for step in range(1, FS_COUNT):
        far_z = lax.rem(z + step // FS_SIDE, FS_SIDE)
        far_x = lax.rem(x + step % FS_SIDE, FS_SIDE)
        yield step, far_z, far_x


def shares_out(parts, landing, send, recv, z, x):
    return [
        pltpu.make_async_remote_copy(
            src_ref=parts.at[far_z * FS_SIDE + far_x],
            dst_ref=landing.at[step],
            send_sem=send.at[step],
            recv_sem=recv.at[step],
            device_id={"fs_0": far_z, "fs_1": far_x},
            device_id_type=MESH,
        )
        for step, far_z, far_x in spread(z, x)
    ]


def rows_out(rows, send, recv, z, x):
    mine = rows.at[z * FS_SIDE + x]
    return [
        pltpu.make_async_remote_copy(
            src_ref=mine,
            dst_ref=mine,
            send_sem=send.at[step],
            recv_sem=recv.at[step],
            device_id={"fs_0": far_z, "fs_1": far_x},
            device_id_type=MESH,
        )
        for step, far_z, far_x in spread(z, x)
    ]


def sums_out(sums, send, recv, y, c):
    return [
        pltpu.make_async_remote_copy(
            src_ref=sums.at[0],
            dst_ref=sums.at[step],
            send_sem=send.at[step],
            recv_sem=recv.at[step],
            device_id={
                "tp_0": lax.rem(y + step // 2, 4),
                "tp_1": lax.rem(c + step % 2, 2),
            },
            device_id_type=MESH,
        )
        for step in range(1, 8)
    ]


def start(copies):
    for copy in copies:
        copy.start()


def arrive(copies):
    for copy in copies:
        copy.wait_recv()


def finish(copies):
    for copy in copies:
        copy.wait_send()


def body(
    lam_ref,
    gain_ref,
    out_weight_ref,
    value_weight_ref,
    out_first_ref,
    out_second_ref,
    value_first_ref,
    value_second_ref,
    query_hbm,
    key_hbm,
    value_hbm,
    out_cot_hbm,
    layer_hbm,
    value_cot_hbm,
    out_basis_hbm,
    value_basis_hbm,
    out_step_ref,
    value_step_ref,
    new_out_weight_ref,
    new_value_weight_ref,
    out_copy_ref,
    value_copy_ref,
    new_out_first_ref,
    new_out_second_ref,
    new_value_first_ref,
    new_value_second_ref,
    query_ref,
    key_ref,
    value_ref,
    value_cot_ref,
    out_basis_ref,
    value_basis_ref,
    layer_ref,
    out_cot_ref,
    turned_ref,
    score_ref,
    weight_ref,
    head_ref,
    high_ref,
    low_ref,
    out_all_ref,
    value_all_ref,
    value_parts,
    value_landing,
    value_rows,
    value_sums,
    out_parts,
    out_landing,
    out_rows,
    out_sums,
    total_ref,
    local_sem,
    gather_out_send,
    gather_out_recv,
    gather_value_send,
    gather_value_recv,
    share_send,
    share_recv,
    row_send,
    row_recv,
    sum_send,
    sum_recv,
):
    z, x = lax.axis_index("fs_0"), lax.axis_index("fs_1")
    y, c = lax.axis_index("tp_0"), lax.axis_index("tp_1")
    me = z * FS_SIDE + x
    chunks = SEQ // BLOCK

    def span(n):
        return slice(n * BLOCK, (n + 1) * BLOCK)

    local = []

    def fetch(src, dst):
        copy = pltpu.make_async_copy(src, dst, local_sem.at[len(local)])
        local.append(copy)
        copy.start()
        return copy

    got_value_basis = fetch(value_basis_hbm, value_basis_ref)
    got_value_cot = fetch(value_cot_hbm, value_cot_ref)
    got_layer = [fetch(layer_hbm.at[span(n)], layer_ref.at[span(n)]) for n in range(chunks)]
    got_qkv = [
        fetch(query_hbm, query_ref),
        fetch(key_hbm, key_ref),
        fetch(value_hbm, value_ref),
    ]
    got_out_basis = fetch(out_basis_hbm, out_basis_ref)
    got_out_cot = [fetch(out_cot_hbm.at[span(n)], out_cot_ref.at[span(n)]) for n in range(chunks)]

    barrier = pltpu.get_barrier_semaphore()
    for _, far_z, far_x in spread(z, x):
        pl.semaphore_signal(
            barrier, inc=1, device_id={"fs_0": far_z, "fs_1": far_x}, device_id_type=MESH
        )
    for step in range(1, 8):
        pl.semaphore_signal(
            barrier,
            inc=1,
            device_id={"tp_0": lax.rem(y + step // 2, 4), "tp_1": lax.rem(c + step % 2, 2)},
            device_id_type=MESH,
        )
    out_all_ref[z, x, 0] = out_weight_ref[:128, :]
    out_all_ref[z, x, 1] = out_weight_ref[128:, :]
    pl.semaphore_wait(barrier, 22)

    gather_out = Gather(out_all_ref, gather_out_send, gather_out_recv, z, x)
    gather_value = Gather(value_all_ref, gather_value_send, gather_value_recv, z, x)
    value_shares = shares_out(value_parts, value_landing, share_send.at[0], share_recv.at[0], z, x)
    out_shares = shares_out(out_parts, out_landing, share_send.at[1], share_recv.at[1], z, x)
    value_row_copies = rows_out(value_rows, row_send.at[0], row_recv.at[0], z, x)
    out_row_copies = rows_out(out_rows, row_send.at[1], row_recv.at[1], z, x)
    value_sum_copies = sums_out(value_sums, sum_send.at[0], sum_recv.at[0], y, c)
    out_sum_copies = sums_out(out_sums, sum_send.at[1], sum_recv.at[1], y, c)

    gather_out.start(0)

    got_value_basis.wait()
    got_value_cot.wait()
    proj_t = None
    for n in range(chunks):
        got_layer[n].wait()
        wide = mul(layer_ref[span(n), :], value_basis_ref[...])
        high, low = two_parts(wide)
        turned = value_cot_ref[span(n), :].T
        part = mul(turned, high) + mul(turned, low)
        proj_t = part if proj_t is None else proj_t + part
    value_parts[...] = proj_t.T.reshape(FS_COUNT, SHARE, COLS)
    start(value_shares)
    gather_out.arrive(0)
    gather_out.start(1)

    for copy in got_qkv:
        copy.wait()
    got_out_basis.wait()
    for n in range(chunks):
        turned_ref[:, span(n)] = value_ref[span(n), :].T
    gain = column(gain_ref[...])
    gain = jnp.concatenate([gain, gain], axis=1)
    lane = lax.broadcasted_iota(jnp.int32, (BLOCK, 128), 1)
    causal = lax.broadcasted_iota(jnp.int32, (BLOCK, BLOCK), 0) <= lax.broadcasted_iota(
        jnp.int32, (BLOCK, BLOCK), 1
    )

    jobs = [(i, h) for i in range(chunks) for h in range(2)]

    def scores(n, peaks):
        i, h = jobs[n]
        both = []
        for m in range(2):
            scaled = query_ref[span(i), h * 128 : (h + 1) * 128].astype(F32) * SCORE_SCALE
            scaled = jnp.where((lane < DH) if m == 0 else (lane >= DH), scaled, 0.0)
            both.append(jnp.concatenate(two_parts(scaled), axis=1))
        best = [None, None]
        for j in range(i + 1):
            keys = key_ref[span(j), h * 128 : (h + 1) * 128]
            for m in range(2):
                s = mul(jnp.concatenate([keys, keys], axis=1), both[m], NT)
                if j == i:
                    s = jnp.where(causal, s, -jnp.inf)
                score_ref[n % 2, m, span(j), :] = s
                top = jnp.max(s.reshape(BLOCK // 8, 8, BLOCK), axis=0)
                best[m] = top if best[m] is None else jnp.maximum(best[m], top)
                yield
        peaks.extend(jnp.max(b, axis=0, keepdims=True) for b in best)

    def weigh(n, peaks):
        i, h = jobs[n]
        held = score_ref.at[n % 2]
        sums = [None, None]
        for j in range(i + 1):
            for m in range(2):
                e = jnp.exp2(held[m, span(j), :] - peaks[m])
                part = jnp.sum(e.reshape(BLOCK // 8, 8, BLOCK), axis=0)
                sums[m] = part if sums[m] is None else sums[m] + part
                held[m, span(j), :] = e
                yield
        sums = [jnp.sum(t, axis=0, keepdims=True) for t in sums]
        one, two = 1.0 / sums[0], lam_ref[h] / sums[1]
        for j in range(i + 1):
            mixed = held[0, span(j), :] * one - held[1, span(j), :] * two
            weight_ref[n % 2, span(j), :] = mixed.astype(BF16)
            yield
        depth = (i + 1) * BLOCK
        raw = mul(turned_ref[h * DV : (h + 1) * DV, :depth], weight_ref[n % 2, :depth, :])
        mean = jnp.mean(raw * raw, axis=0, keepdims=True)
        normed = raw * lax.rsqrt(mean + EPSILON_NORM) * gain
        head_ref[h * DV : (h + 1) * DV, span(i)] = normed.astype(BF16)

    def together(first, first_count, second, second_count):
        due = 0.0
        for _ in range(first_count):
            next(first, None)
            due += second_count / first_count
            while due >= 1.0:
                next(second, None)
                due -= 1.0
        for chain in (first, second):
            for _ in chain:
                pass

    def clip_of(sums):
        total = jnp.sum(sums[...], axis=0)[0:1, 0:1]
        return jnp.minimum(1.0, CLIP_RMS * math.sqrt(ENTRY_COUNT) / jnp.sqrt(total))

    def moments(parts, landing, first, second, new_first, new_second, rows):
        proj = parts[me]
        for step in range(1, FS_COUNT):
            proj = proj + landing[step]
        new_first[...], new_second[...], direction = moment_step(proj, first[...], second[...])
        rows[me] = direction

    def square_sum(rows, sums):
        every = rows[...].reshape(RANK, COLS)
        sums[0] = jnp.broadcast_to(jnp.sum(every * every, keepdims=True), (8, 128))

    def after(job):
        if job == 3:
            gather_out.arrive(1)
            gather_out.start(2)
        if job == 6:
            arrive(value_shares)
            moments(
                value_parts,
                value_landing,
                value_first_ref,
                value_second_ref,
                new_value_first_ref,
                new_value_second_ref,
                value_rows,
            )
            start(value_row_copies)
        if job == 9:
            arrive(value_row_copies)
            square_sum(value_rows, value_sums)
            start(value_sum_copies)
        if job == 10:
            gather_out.arrive(2)
            gather_out.start(3)
        if job == 11:
            arrive(value_sum_copies)
            high, low = two_parts(value_rows[...].reshape(RANK, COLS))
            own = value_basis_ref[pl.ds(pl.multiple_of(me * OWN, OWN), OWN), :]
            step = clip_of(value_sums) * (mul(own, high) + mul(own, low))
            value_step_ref[...] = step
            new = value_weight_ref[...] - LEARN_RATE * step
            new_value_weight_ref[...] = new
            value_all_ref[z, x] = new.astype(BF16).reshape(2, OWN // 2, COLS)
            gather_value.start(0)
        if job == 12:
            gather_value.arrive(0)
            gather_value.start(1)
        if job == 13:
            gather_value.arrive(1)
            gather_value.start(2)
        if job == 15:
            gather_value.arrive(2)
            gather_value.start(3)

    peaks = [[] for _ in jobs]
    for _ in scores(0, peaks[0]):
        pass
    for n, (i, h) in enumerate(jobs):
        if h == 0:
            got_out_cot[i].wait()
            wide = mul(out_cot_ref[span(i), :], out_basis_ref[...])
            high_ref[span(i), :], low_ref[span(i), :] = two_parts(wide)
        ahead, ahead_count = iter(()), 0
        if n + 1 < len(jobs):
            ahead, ahead_count = scores(n + 1, peaks[n + 1]), 2 * (jobs[n + 1][0] + 1) + 1
        together(weigh(n, peaks[n]), 3 * (i + 1) + 1, ahead, ahead_count)
        after(n)

    proj_t = mul(head_ref[...], high_ref[...]) + mul(head_ref[...], low_ref[...])
    out_parts[...] = proj_t.T.reshape(FS_COUNT, SHARE, COLS)
    start(out_shares)
    arrive(out_shares)
    moments(
        out_parts,
        out_landing,
        out_first_ref,
        out_second_ref,
        new_out_first_ref,
        new_out_second_ref,
        out_rows,
    )
    start(out_row_copies)
    gather_out.arrive(3)
    gather_value.arrive(3)
    for at in range(FS_COUNT):
        value_copy_ref[at * OWN : (at + 1) * OWN, :] = value_all_ref[
            at // FS_SIDE, at % FS_SIDE
        ].reshape(OWN, COLS)
    arrive(out_row_copies)
    square_sum(out_rows, out_sums)
    start(out_sum_copies)
    high, low = two_parts(out_rows[...].reshape(RANK, COLS).T)
    for at in range(FS_COUNT):
        basis = out_basis_ref[at * OWN : (at + 1) * OWN, :]
        total_ref[at] = mul(high, basis, NT) + mul(low, basis, NT)
    arrive(out_sum_copies)
    clip = clip_of(out_sums)
    step = clip * total_ref[me]
    out_step_ref[...] = step
    new_out_weight_ref[...] = out_weight_ref[...] - LEARN_RATE * step
    for at in range(FS_COUNT):
        old = out_all_ref[at // FS_SIDE, at % FS_SIDE].reshape(COLS, OWN)
        new = old - LEARN_RATE * (clip * total_ref[at])
        out_copy_ref[:, at * OWN : (at + 1) * OWN] = new.astype(BF16)

    gather_out.finish()
    gather_value.finish()
    for copies in (
        value_shares,
        out_shares,
        value_row_copies,
        out_row_copies,
        value_sum_copies,
        out_sum_copies,
    ):
        finish(copies)


def step(
    query_rows,
    key_rows,
    value_rows,
    mix_lambda,
    head_gain,
    out_cotangent,
    layer_input,
    value_cotangent,
    out_weight,
    value_weight,
    out_basis,
    value_basis,
    out_first,
    out_second,
    value_first,
    value_second,
):
    vmem = pl.BlockSpec(memory_space=pltpu.VMEM)
    smem = pl.BlockSpec(memory_space=pltpu.SMEM)
    anywhere = pl.BlockSpec(memory_space=pl.ANY)
    dma = pltpu.SemaphoreType.DMA
    shape = jax.ShapeDtypeStruct
    return pl.pallas_call(
        body,
        out_shape=(
            shape((COLS, OWN), F32),
            shape((OWN, COLS), F32),
            shape((COLS, OWN), F32),
            shape((OWN, COLS), F32),
            shape((COLS, WIDE), BF16),
            shape((WIDE, COLS), BF16),
            shape((SHARE, COLS), F32),
            shape((SHARE, COLS), F32),
            shape((SHARE, COLS), F32),
            shape((SHARE, COLS), F32),
        ),
        in_specs=[smem] + [vmem] * 7 + [anywhere] * 8,
        out_specs=(vmem,) * 10,
        scratch_shapes=[
            pltpu.VMEM((SEQ, COLS), BF16),
            pltpu.VMEM((SEQ, COLS), BF16),
            pltpu.VMEM((SEQ, COLS), BF16),
            pltpu.VMEM((SEQ, COLS), BF16),
            pltpu.VMEM((WIDE, RANK), BF16),
            pltpu.VMEM((WIDE, RANK), BF16),
            pltpu.VMEM((SEQ, WIDE), BF16),
            pltpu.VMEM((SEQ, WIDE), BF16),
            pltpu.VMEM((COLS, SEQ), BF16),
            pltpu.VMEM((2, 2, SEQ, BLOCK), F32),
            pltpu.VMEM((2, SEQ, BLOCK), BF16),
            pltpu.VMEM((COLS, SEQ), BF16),
            pltpu.VMEM((SEQ, RANK), BF16),
            pltpu.VMEM((SEQ, RANK), BF16),
            pltpu.VMEM((FS_SIDE, FS_SIDE, 2, COLS // 2, OWN), F32),
            pltpu.VMEM((FS_SIDE, FS_SIDE, 2, OWN // 2, COLS), BF16),
            pltpu.VMEM((FS_COUNT, SHARE, COLS), F32),
            pltpu.VMEM((FS_COUNT, SHARE, COLS), F32),
            pltpu.VMEM((FS_COUNT, SHARE, COLS), F32),
            pltpu.VMEM((8, 8, 128), F32),
            pltpu.VMEM((FS_COUNT, SHARE, COLS), F32),
            pltpu.VMEM((FS_COUNT, SHARE, COLS), F32),
            pltpu.VMEM((FS_COUNT, SHARE, COLS), F32),
            pltpu.VMEM((8, 8, 128), F32),
            pltpu.VMEM((FS_COUNT, COLS, OWN), F32),
            dma((32,)),
            dma((16,)),
            dma((16,)),
            dma((16,)),
            dma((16,)),
            dma((2, 16)),
            dma((2, 16)),
            dma((2, 16)),
            dma((2, 16)),
            dma((2, 8)),
            dma((2, 8)),
        ],
        compiler_params=pltpu.CompilerParams(
            collective_id=0, has_side_effects=True, vmem_limit_bytes=62 * 2**20
        ),
    )(
        mix_lambda,
        head_gain.reshape(1, DV),
        out_weight,
        value_weight,
        out_first,
        out_second,
        value_first,
        value_second,
        query_rows,
        key_rows,
        value_rows,
        out_cotangent,
        layer_input,
        value_cotangent,
        out_basis,
        value_basis,
    )


def solution(mesh):
    torus = Mesh(mesh.devices.reshape(4, 4, 4, 2), FS + TP)
    sliced = P(FS, TP)
    return jax.shard_map(
        step,
        mesh=torus,
        in_specs=(
            sliced,
            sliced,
            sliced,
            P(TP),
            P(),
            P(FS, None),
            P(FS, None),
            sliced,
            P(TP, FS),
            sliced,
            P(),
            P(),
            sliced,
            sliced,
            sliced,
            sliced,
        ),
        out_specs=(
            P(TP, FS),
            sliced,
            P(TP, FS),
            sliced,
            P(TP, None),
            P(None, TP),
            sliced,
            sliced,
            sliced,
            sliced,
        ),
        check_vma=False,
    )
```

time: 271 us -> 88.1 us (0.33)
  matrix products: 88.5 us -> 0 us
  Pallas kernels: 0 us -> 69.8 us
  blocking collectives: 54.9 us -> 0 us
  other arithmetic: 53.4 us -> 0 us
  waiting for transfers between devices: 28.1 us -> 0 us
  starting transfers between devices: 23.1 us -> 0 us
  loops' own time: 2.95 us -> 0 us
    pallas_call x0 -> x1, Pallas kernels: none -> 69.8 us  [step(): pl.pallas_call(body, out_shape=(shape((COLS, OWN), F32), shape((OWN, COLS...]
    div x4 -> x0, other arithmetic: 47.8 us -> none  [one_block(): soft_maps = exp_scores / jnp.sum(exp_scores, axis=-1, keepdims=True)]
    dot_general x10 -> x0, matrix products: 47.2 us -> none  [the longest x4 27.2 us: one_block(): jnp.einsum('hqk,khv->qhv', mix_weights, value_three, preferred_element_ty...]
    sub x4 -> x0, matrix products: 41.3 us -> none  [one_block(): exp_scores = jnp.exp(scores - row_peak)]
    psum x4 -> x0, blocking collectives: 32.9 us -> none  [by_axis(): return functools.reduce(lax.psum, axes, value)]
    all_to_all x4 -> x0, waiting for transfers between devices: 28.1 us -> none  [the longest x2 20.4 us: sent_to_all(): lax.all_to_all(jnp.broadcast_to(value[None], (count, *value.shape)), axis...]
    all_to_all x4 -> x0, starting transfers between devices: 23.1 us -> none  [the longest x2 14.9 us: sum_at_owner(): tiles = lax.all_to_all(in_blocks(value, dim, count), axis, 0, 0, tiled=True)]
    all_gather x1 -> x0, blocking collectives: 21.9 us -> none  [sent_together(): lax.all_gather(both, axis, axis=dim, tiled=True)]
  transfers between devices with their start and end apart: 4 -> 0, of which waited for: 4 -> 0; matrix products, arithmetic and copies ran while one was open for 6% -> 0% of each run, Pallas kernels for 0% -> 0%
where the time goes in v1:
time: 88.1 us; the launch traced here: 86.6 us
  Pallas kernels  69.8 us (79%)
  local copies, waits for them, and re-layouts  16.1 us (18%)
    pallas_call x1, Pallas kernels, step(): pl.pallas_call(body, out_shape=(shape((COLS, OWN), F32), shape((OWN, COLS...  69.8 us
    unnamed x10, local copies, waits for them, and re-layouts  16.1 us

profile of v1, /device:TPU:0, one launch (start us, length us, event | category | flops | bytes accessed | tf_op | source)
XLA Modules:
  0.0 86.6 jit_solution(5930969595777713676)
XLA Ops:
  0.6 69.8 %shard_map.231 = (f32[256,128]{1,0:T(8,128)}, f32[128,256]{1,0:T(8,128)}, f32[256,128]{1,0:T(8,128)}, f32[128,256]{1,0:T(8,128)}, bf16[256,2048]{1,0:T(8,128)(2,...) custom-call(f32[2]{0:T(128)} %lam_ref.1, ...), custom_call_target="tpu_custom_call" | custom-call | tf_op jit(solution)/shard_map/pallas_call | solution.py:532
  70.4 1.6 %copy.36 = f32[256,128]{1,0:T(8,128)} copy(f32[256,128]{1,0:T(8,128)} %get-tuple-element.20) | data formatting | bytes 262144
  72.0 1.6 %copy.37 = f32[128,256]{1,0:T(8,128)} copy(f32[128,256]{1,0:T(8,128)} %get-tuple-element.21) | data formatting | bytes 262144
  73.6 1.6 %copy.38 = f32[256,128]{1,0:T(8,128)} copy(f32[256,128]{1,0:T(8,128)} %get-tuple-element.22) | data formatting | bytes 262144
  75.1 1.6 %copy.39 = f32[128,256]{1,0:T(8,128)} copy(f32[128,256]{1,0:T(8,128)} %get-tuple-element.23) | data formatting | bytes 262144
  76.7 2.3 %copy.40 = bf16[256,2048]{1,0:T(8,128)(2,1)} copy(bf16[256,2048]{1,0:T(8,128)(2,1)} %get-tuple-element.24) | data formatting | bytes 2097152
  79.0 2.3 %copy.41 = bf16[2048,256]{1,0:T(8,128)(2,1)} copy(bf16[2048,256]{1,0:T(8,128)(2,1)} %get-tuple-element.25) | data formatting | bytes 2097152
  81.3 1.3 %copy.42 = f32[16,256]{1,0:T(8,128)} copy(f32[16,256]{1,0:T(8,128)} %get-tuple-element.26) | data formatting | bytes 32768
  82.6 1.3 %copy.43 = f32[16,256]{1,0:T(8,128)} copy(f32[16,256]{1,0:T(8,128)} %get-tuple-element.27) | data formatting | bytes 32768
  83.9 1.3 %copy.44 = f32[16,256]{1,0:T(8,128)} copy(f32[16,256]{1,0:T(8,128)} %get-tuple-element.28) | data formatting | bytes 32768
  85.2 1.3 %copy.45 = f32[16,256]{1,0:T(8,128)} copy(f32[16,256]{1,0:T(8,128)} %get-tuple-element.29) | data formatting | bytes 32768

commit v2 on v1

--- a/solution.py
+++ b/solution.py
@@ -164,6 +164,20 @@
             device_id_type=MESH,
         )
         for step in range(1, 8)
+    ]
+
+
+def totals_out(totals, send, recv, z, x):
+    return [
+        pltpu.make_async_remote_copy(
+            src_ref=totals.at[0],
+            dst_ref=totals.at[step],
+            send_sem=send.at[step],
+            recv_sem=recv.at[step],
+            device_id={"fs_0": far_z, "fs_1": far_x},
+            device_id_type=MESH,
+        )
+        for step, far_z, far_x in spread(z, x)
     ]
 
 
@@ -224,16 +238,18 @@
     high_ref,
     low_ref,
     out_all_ref,
-    value_all_ref,
     value_parts,
     value_landing,
     value_rows,
     value_sums,
+    value_totals,
     out_parts,
     out_landing,
     out_rows,
     out_sums,
-    total_ref,
+    out_totals,
+    out_full_ref,
+    proj_ref,
     local_sem,
     gather_out_send,
     gather_out_recv,
@@ -245,6 +261,8 @@
     row_recv,
     sum_send,
     sum_recv,
+    total_send,
+    total_recv,
 ):
     z, x = lax.axis_index("fs_0"), lax.axis_index("fs_1")
     y, c = lax.axis_index("tp_0"), lax.axis_index("tp_1")
@@ -262,17 +280,20 @@
         copy.start()
         return copy
 
+    def part(n):
+        return slice(n * 2 * BLOCK, (n + 1) * 2 * BLOCK)
+
     got_value_basis = fetch(value_basis_hbm, value_basis_ref)
+    got_layer = [fetch(layer_hbm.at[part(0)], layer_ref.at[part(0)])]
     got_value_cot = fetch(value_cot_hbm, value_cot_ref)
-    got_layer = [fetch(layer_hbm.at[span(n)], layer_ref.at[span(n)]) for n in range(chunks)]
+    for n in range(1, chunks // 2):
+        got_layer.append(fetch(layer_hbm.at[part(n)], layer_ref.at[part(n)]))
     got_qkv = [
         fetch(query_hbm, query_ref),
         fetch(key_hbm, key_ref),
         fetch(value_hbm, value_ref),
     ]
     got_out_basis = fetch(out_basis_hbm, out_basis_ref)
-    got_out_cot = [fetch(out_cot_hbm.at[span(n)], out_cot_ref.at[span(n)]) for n in range(chunks)]
-
     barrier = pltpu.get_barrier_semaphore()
     for _, far_z, far_x in spread(z, x):
         pl.semaphore_signal(
@@ -287,39 +308,45 @@
         )
     out_all_ref[z, x, 0] = out_weight_ref[:128, :]
     out_all_ref[z, x, 1] = out_weight_ref[128:, :]
-    pl.semaphore_wait(barrier, 22)
 
     gather_out = Gather(out_all_ref, gather_out_send, gather_out_recv, z, x)
-    gather_value = Gather(value_all_ref, gather_value_send, gather_value_recv, z, x)
+    gather_value = Gather(value_copy_ref, gather_value_send, gather_value_recv, z, x)
+    gathers = (gather_out, gather_value)
     value_shares = shares_out(value_parts, value_landing, share_send.at[0], share_recv.at[0], z, x)
     out_shares = shares_out(out_parts, out_landing, share_send.at[1], share_recv.at[1], z, x)
     value_row_copies = rows_out(value_rows, row_send.at[0], row_recv.at[0], z, x)
     out_row_copies = rows_out(out_rows, row_send.at[1], row_recv.at[1], z, x)
     value_sum_copies = sums_out(value_sums, sum_send.at[0], sum_recv.at[0], y, c)
     out_sum_copies = sums_out(out_sums, sum_send.at[1], sum_recv.at[1], y, c)
-
-    gather_out.start(0)
+    value_total_copies = totals_out(value_totals, total_send.at[0], total_recv.at[0], z, x)
+    out_total_copies = totals_out(out_totals, total_send.at[1], total_recv.at[1], z, x)
 
     got_value_basis.wait()
-    got_value_cot.wait()
-    proj_t = None
-    for n in range(chunks):
+    for n in range(chunks // 2):
         got_layer[n].wait()
-        wide = mul(layer_ref[span(n), :], value_basis_ref[...])
-        high, low = two_parts(wide)
-        turned = value_cot_ref[span(n), :].T
-        part = mul(turned, high) + mul(turned, low)
-        proj_t = part if proj_t is None else proj_t + part
+        if n == 1:
+            got_value_cot.wait()
+            pl.semaphore_wait(barrier, 22)
+            gather_out.start(0)
+        if n == 3:
+            got_out_cot = [
+                fetch(out_cot_hbm.at[span(t)], out_cot_ref.at[span(t)]) for t in range(chunks)
+            ]
+        wide = mul(layer_ref[part(n), :], value_basis_ref[...])
+        high_ref[part(n), :], low_ref[part(n), :] = two_parts(wide)
+        if n == 1:
+            for t in range(chunks):
+                head_ref[:, span(t)] = value_cot_ref[span(t), :].T
+    proj_t = mul(head_ref[...], high_ref[...]) + mul(head_ref[...], low_ref[...])
     value_parts[...] = proj_t.T.reshape(FS_COUNT, SHARE, COLS)
-    start(value_shares)
     gather_out.arrive(0)
     gather_out.start(1)
+    start(value_shares)
 
     for copy in got_qkv:
         copy.wait()
     got_out_basis.wait()
-    for n in range(chunks):
-        turned_ref[:, span(n)] = value_ref[span(n), :].T
+    turned_ref[:, span(0)] = value_ref[span(0), :].T
     gain = column(gain_ref[...])
     gain = jnp.concatenate([gain, gain], axis=1)
     lane = lax.broadcasted_iota(jnp.int32, (BLOCK, 128), 1)
@@ -384,26 +411,28 @@
             for _ in chain:
                 pass
 
-    def clip_of(sums):
-        total = jnp.sum(sums[...], axis=0)[0:1, 0:1]
+    def clip_of(totals):
+        total = jnp.sum(jnp.sum(totals[...], axis=0), keepdims=True)
         return jnp.minimum(1.0, CLIP_RMS * math.sqrt(ENTRY_COUNT) / jnp.sqrt(total))
 
-    def moments(parts, landing, first, second, new_first, new_second, rows):
+    def moments(parts, landing, first, second, new_first, new_second, rows, sums):
         proj = parts[me]
         for step in range(1, FS_COUNT):
             proj = proj + landing[step]
         new_first[...], new_second[...], direction = moment_step(proj, first[...], second[...])
         rows[me] = direction
-
-    def square_sum(rows, sums):
-        every = rows[...].reshape(RANK, COLS)
-        sums[0] = jnp.broadcast_to(jnp.sum(every * every, keepdims=True), (8, 128))
-
-    def after(job):
-        if job == 3:
-            gather_out.arrive(1)
-            gather_out.start(2)
-        if job == 6:
+        square = direction * direction
+        sums[0] = square[:8, :128] + square[8:, :128] + square[:8, 128:] + square[8:, 128:]
+
+    def gather_next(gather, stage):
+        gather.arrive(stage)
+        if stage < 3:
+            gather.start(stage + 1)
+
+    def after(n):
+        if n == 4:
+            gather_next(gather_out, 1)
+        if n == 7:
             arrive(value_shares)
             moments(
                 value_parts,
@@ -413,52 +442,67 @@
                 new_value_first_ref,
                 new_value_second_ref,
                 value_rows,
+                value_sums,
             )
+            start(value_sum_copies)
             start(value_row_copies)
-        if job == 9:
+        if n == 10:
+            arrive(value_sum_copies)
+            value_totals[0] = jnp.sum(value_sums[...], axis=0)
+            start(value_total_copies)
+        if n == 12:
+            gather_next(gather_out, 2)
+        if n == 14:
             arrive(value_row_copies)
-            square_sum(value_rows, value_sums)
-            start(value_sum_copies)
-        if job == 10:
-            gather_out.arrive(2)
-            gather_out.start(3)
-        if job == 11:
-            arrive(value_sum_copies)
+            arrive(value_total_copies)
             high, low = two_parts(value_rows[...].reshape(RANK, COLS))
             own = value_basis_ref[pl.ds(pl.multiple_of(me * OWN, OWN), OWN), :]
-            step = clip_of(value_sums) * (mul(own, high) + mul(own, low))
+            step = clip_of(value_totals) * (mul(own, high) + mul(own, low))
             value_step_ref[...] = step
             new = value_weight_ref[...] - LEARN_RATE * step
             new_value_weight_ref[...] = new
-            value_all_ref[z, x] = new.astype(BF16).reshape(2, OWN // 2, COLS)
+            value_copy_ref[z, x] = new.astype(BF16).reshape(2, OWN // 2, COLS)
             gather_value.start(0)
-        if job == 12:
-            gather_value.arrive(0)
-            gather_value.start(1)
-        if job == 13:
-            gather_value.arrive(1)
-            gather_value.start(2)
-        if job == 15:
-            gather_value.arrive(2)
-            gather_value.start(3)
+
+    def widen(n):
+        wide = mul(out_cot_ref[span(n), :], out_basis_ref[...])
+        high_ref[span(n), :], low_ref[span(n), :] = two_parts(wide)
+
+    def project(low, high):
+        rows = slice(low * BLOCK, high * BLOCK)
+        return mul(head_ref[:, rows], high_ref[rows, :]) + mul(head_ref[:, rows], low_ref[rows, :])
+
+    wide_at = {3: 0, 5: 1, 7: 2, 8: 3, 9: 4, 10: 5, 11: 6, 12: 7}
+
+    def extra(n):
+        i, h = jobs[n]
+        if n in wide_at:
+            widen(wide_at[n])
+        if n == 13:
+            proj_ref[...] = project(0, 5)
+        if n == 15:
+            proj_ref[...] += project(5, 7)
+        if h == 1 and i + 1 < chunks:
+            turned_ref[:, span(i + 1)] = value_ref[span(i + 1), :].T
 
     peaks = [[] for _ in jobs]
     for _ in scores(0, peaks[0]):
         pass
     for n, (i, h) in enumerate(jobs):
-        if h == 0:
-            got_out_cot[i].wait()
-            wide = mul(out_cot_ref[span(i), :], out_basis_ref[...])
-            high_ref[span(i), :], low_ref[span(i), :] = two_parts(wide)
+        if n in wide_at:
+            got_out_cot[wide_at[n]].wait()
+        extra(n)
         ahead, ahead_count = iter(()), 0
         if n + 1 < len(jobs):
             ahead, ahead_count = scores(n + 1, peaks[n + 1]), 2 * (jobs[n + 1][0] + 1) + 1
         together(weigh(n, peaks[n]), 3 * (i + 1) + 1, ahead, ahead_count)
         after(n)
 
-    proj_t = mul(head_ref[...], high_ref[...]) + mul(head_ref[...], low_ref[...])
+    proj_t = proj_ref[...] + project(7, 8)
     out_parts[...] = proj_t.T.reshape(FS_COUNT, SHARE, COLS)
     start(out_shares)
+    gather_next(gather_value, 0)
+    gather_next(gather_value, 1)
     arrive(out_shares)
     moments(
         out_parts,
@@ -468,33 +512,35 @@
         new_out_first_ref,
         new_out_second_ref,
         out_rows,
+        out_sums,
     )
+    start(out_sum_copies)
     start(out_row_copies)
-    gather_out.arrive(3)
-    gather_value.arrive(3)
-    for at in range(FS_COUNT):
-        value_copy_ref[at * OWN : (at + 1) * OWN, :] = value_all_ref[
-            at // FS_SIDE, at % FS_SIDE
-        ].reshape(OWN, COLS)
+    arrive(out_sum_copies)
+    out_totals[0] = jnp.sum(out_sums[...], axis=0)
+    start(out_total_copies)
+    gather_next(gather_value, 2)
+    gather_next(gather_out, 3)
     arrive(out_row_copies)
-    square_sum(out_rows, out_sums)
-    start(out_sum_copies)
-    high, low = two_parts(out_rows[...].reshape(RANK, COLS).T)
-    for at in range(FS_COUNT):
-        basis = out_basis_ref[at * OWN : (at + 1) * OWN, :]
-        total_ref[at] = mul(high, basis, NT) + mul(low, basis, NT)
-    arrive(out_sum_copies)
-    clip = clip_of(out_sums)
-    step = clip * total_ref[me]
+    both = jnp.concatenate(two_parts(out_rows[...].reshape(RANK, COLS).T), axis=0)
+    for n in range(chunks):
+        full = mul(both, out_basis_ref[span(n), :], NT)
+        out_full_ref[:, span(n)] = full[:COLS] + full[COLS:]
+    arrive(out_total_copies)
+    clip = clip_of(out_totals)
+    own = pl.ds(pl.multiple_of(me * OWN, OWN), OWN)
+    step = clip * out_full_ref[:, own]
     out_step_ref[...] = step
     new_out_weight_ref[...] = out_weight_ref[...] - LEARN_RATE * step
     for at in range(FS_COUNT):
         old = out_all_ref[at // FS_SIDE, at % FS_SIDE].reshape(COLS, OWN)
-        new = old - LEARN_RATE * (clip * total_ref[at])
-        out_copy_ref[:, at * OWN : (at + 1) * OWN] = new.astype(BF16)
-
-    gather_out.finish()
-    gather_value.finish()
+        cols = slice(at * OWN, (at + 1) * OWN)
+        new = old - LEARN_RATE * (clip * out_full_ref[:, cols])
+        out_copy_ref[:, cols] = new.astype(BF16)
+
+    gather_next(gather_value, 3)
+    for gather in gathers:
+        gather.finish()
     for copies in (
         value_shares,
         out_shares,
@@ -502,8 +548,36 @@
         out_row_copies,
         value_sum_copies,
         out_sum_copies,
+        value_total_copies,
+        out_total_copies,
     ):
         finish(copies)
+
+
+def hand_over(*refs):
+    count = len(refs) // 3
+    given, taken, held = refs[:count], refs[count : 2 * count], refs[2 * count : 3 * count]
+    sems = refs[3 * count]
+    loads = [pltpu.make_async_copy(a, b, sems.at[0, n]) for n, (a, b) in enumerate(zip(given, held))]
+    stores = [pltpu.make_async_copy(a, b, sems.at[1, n]) for n, (a, b) in enumerate(zip(held, taken))]
+    start(loads)
+    for load, store in zip(loads, stores):
+        load.wait()
+        store.start()
+    for store in stores:
+        store.wait()
+
+
+def results(arrays):
+    anywhere = pl.BlockSpec(memory_space=pl.ANY)
+    return pl.pallas_call(
+        hand_over,
+        out_shape=tuple(jax.ShapeDtypeStruct(a.shape, a.dtype) for a in arrays),
+        in_specs=[anywhere] * len(arrays),
+        out_specs=(anywhere,) * len(arrays),
+        scratch_shapes=[pltpu.VMEM(a.shape, a.dtype) for a in arrays]
+        + [pltpu.SemaphoreType.DMA((2, len(arrays)))],
+    )(*arrays)
 
 
 def step(
@@ -529,7 +603,7 @@
     anywhere = pl.BlockSpec(memory_space=pl.ANY)
     dma = pltpu.SemaphoreType.DMA
     shape = jax.ShapeDtypeStruct
-    return pl.pallas_call(
+    arrays = pl.pallas_call(
         body,
         out_shape=(
             shape((COLS, OWN), F32),
@@ -537,7 +611,7 @@
             shape((COLS, OWN), F32),
             shape((OWN, COLS), F32),
             shape((COLS, WIDE), BF16),
-            shape((WIDE, COLS), BF16),
+            shape((FS_SIDE, FS_SIDE, 2, OWN // 2, COLS), BF16),
             shape((SHARE, COLS), F32),
             shape((SHARE, COLS), F32),
             shape((SHARE, COLS), F32),
@@ -561,16 +635,18 @@
             pltpu.VMEM((SEQ, RANK), BF16),
             pltpu.VMEM((SEQ, RANK), BF16),
             pltpu.VMEM((FS_SIDE, FS_SIDE, 2, COLS // 2, OWN), F32),
-            pltpu.VMEM((FS_SIDE, FS_SIDE, 2, OWN // 2, COLS), BF16),
             pltpu.VMEM((FS_COUNT, SHARE, COLS), F32),
             pltpu.VMEM((FS_COUNT, SHARE, COLS), F32),
             pltpu.VMEM((FS_COUNT, SHARE, COLS), F32),
             pltpu.VMEM((8, 8, 128), F32),
+            pltpu.VMEM((FS_COUNT, 8, 128), F32),
             pltpu.VMEM((FS_COUNT, SHARE, COLS), F32),
             pltpu.VMEM((FS_COUNT, SHARE, COLS), F32),
             pltpu.VMEM((FS_COUNT, SHARE, COLS), F32),
             pltpu.VMEM((8, 8, 128), F32),
-            pltpu.VMEM((FS_COUNT, COLS, OWN), F32),
+            pltpu.VMEM((FS_COUNT, 8, 128), F32),
+            pltpu.VMEM((COLS, WIDE), F32),
+            pltpu.VMEM((COLS, RANK), F32),
             dma((32,)),
             dma((16,)),
             dma((16,)),
@@ -582,6 +658,8 @@
             dma((2, 16)),
             dma((2, 8)),
             dma((2, 8)),
+            dma((2, 16)),
+            dma((2, 16)),
         ],
         compiler_params=pltpu.CompilerParams(
             collective_id=0, has_side_effects=True, vmem_limit_bytes=62 * 2**20
@@ -604,6 +682,8 @@
         out_basis,
         value_basis,
     )
+    copy = arrays[5].reshape(WIDE, COLS)
+    return results((*arrays[:5], copy, *arrays[6:]))
 
 
 def solution(mesh):

time: 88.1 us -> 57.7 us (0.65); the launches traced: 86.6 us -> 57.5 us
  local copies, waits for them, and re-layouts: 16.1 us -> 0 us
  Pallas kernels: 69.8 us -> 56.7 us
    unnamed x10 -> x0, local copies, waits for them, and re-layouts: 16.1 us -> none
    pallas_call x1, Pallas kernels: 69.8 us -> 53.7 us  [step(): pl.pallas_call(body, out_shape=(shape((COLS, OWN), F32), shape((OWN, COLS...]
    pallas_call x0 -> x1, Pallas kernels: none -> 3 us  [results(): pl.pallas_call(hand_over, out_shape=tuple((jax.ShapeDtypeStruct(a.shape,...]
where the time goes in v2:
time: 57.7 us; the launch traced here: 57.5 us
  Pallas kernels  56.7 us (98%)
  between operations  0.82 us (1%)
    pallas_call x1, Pallas kernels, step(): pl.pallas_call(body, out_shape=(shape((COLS, OWN), F32), shape((OWN, COLS...  53.7 us
    pallas_call x1, Pallas kernels, results(): pl.pallas_call(hand_over, out_shape=tuple((jax.ShapeDtypeStruct(a.shape,...  3 us

profile of v2, /device:TPU:0, one launch (start us, length us, event | category | flops | bytes accessed | tf_op | source)
XLA Modules:
  0.0 57.5 jit_solution(16687099201692345412)
XLA Ops:
  0.6 53.7 %shard_map.231 = (f32[256,128]{1,0:T(8,128)}, f32[128,256]{1,0:T(8,128)}, f32[256,128]{1,0:T(8,128)}, f32[128,256]{1,0:T(8,128)}, bf16[256,2048]{1,0:T(8,128)(2,...) custom-call(f32[2]{0:T(128)} %lam_ref.1, ...), custom_call_target="tpu_custom_call" | custom-call | tf_op jit(solution)/shard_map/pallas_call | solution.py:606
  54.4 3.0 %shard_map.232 = (f32[256,128]{1,0:T(8,128)}, f32[128,256]{1,0:T(8,128)}, f32[256,128]{1,0:T(8,128)}, f32[128,256]{1,0:T(8,128)}, bf16[256,2048]{1,0:T(8,128)(2,...) custom-call(f32[256,128]{1,0:T(8,128)} %get-tuple-element.20.refs_0_, ...), custom_call_target="tpu_custom_call" | custom-call | tf_op jit(solution)/shard_map/pallas_call | solution.py:573
